TPU v7x, 256 devices: a whole 4x4x8 slice. The times are simulated.
256 devices in a mesh: fs: 32 (over z, x), tp: 8 (over y, core).
Axes of the slice: x: 4, y: 4, z: 8, core: 2. Of those that a mesh axis runs over, the one named last changes fastest.
Arguments:
- saved_input: bfloat16 [393216, 2048], P(('fs', 'tp')), may hold values from -6 to 6
- value_cotangent: bfloat16 [393216, 1024], P(('fs', 'tp')), may hold values from -0.0390625 to 0.0390625
- decay_cotangent: bfloat16 [393216, 16], P(('fs', 'tp')), may hold values from -0.009765625 to 0.009765625
- value_master: float32 [2048, 1024], P('fs', 'tp'), may hold values from -6 to 6
- value_factor: bfloat16 [2048, 256], P('fs'), may hold values from -0.22097087 to 0.22097087
- value_mean: float32 [256, 1024], P('fs', 'tp'), may hold values from -0.625 to 0.625
- value_second: float32 [256, 1024], P('fs', 'tp'), may hold values from 0.0001 to 0.1
- decay_master: float32 [2048, 16], replicated, may hold values from -6 to 6
- decay_mean: float32 [2048, 16], replicated, may hold values from -0.625 to 0.625
- decay_second: float32 [2048, 16], replicated, may hold values from 0.001 to 0.01
Outputs:
- value_step: float32 [2048, 1024], P('fs', 'tp')
- value_new: float32 [2048, 1024], P('fs', 'tp')
- value_copy: bfloat16 [2048, 1024], P(None, 'tp')
- mean_new: float32 [256, 1024], P('fs', 'tp')
- second_new: float32 [256, 1024], P('fs', 'tp')
- decay_step: float32 [2048, 16], replicated
- decay_copy: bfloat16 [2048, 16], replicated
All inputs are finite; a program needn't handle non-finite values.
Results may differ from a plain program's by a relative error of at most 0.0004.
Values may be sent and summed in bfloat16 or wider, within the bound.
A program may use at most 64 MiB of HBM per device.

v0:
```python
import jax
import jax.numpy as jnp
from jax import lax
from jax.sharding import Mesh
from jax.sharding import PartitionSpec as P

D = 2048
GW = 1024
TP = ("tp_0", "tp_1")
FS = ("fs_0", "fs_1")
FS_TP = ("fs_0", "fs_1", "tp_0", "tp_1")


BETA_ONE = 0.9
BETA_TWO = 0.99
ADAM_EPS = 1e-08
RMS_EPS = 1e-06
LEARN_RATE = 0.05
TOKEN_DIMS = (((0,), (0,)), ((), ()))


def split_up(array, dim, devices):
    dims = array.shape
    parts = array.reshape(*dims[:dim], devices, dims[dim] // devices, *dims[dim + 1 :])
    return jnp.moveaxis(parts, dim, 0)


def sent_and_summed(array, axis, dim):
    parts = split_up(array, dim, lax.axis_size(axis))
    arrived = lax.all_to_all(parts, axis, split_axis=0, concat_axis=0, tiled=True)
    return arrived.sum(axis=0)


def sum_in_two_steps(array, axes, dim):
    far, near = axes
    parts = split_up(array, dim, lax.axis_size(far))
    nearer = sent_and_summed(parts, near, dim + 1)
    arrived = lax.all_to_all(nearer, far, split_axis=0, concat_axis=0, tiled=True)
    return arrived.sum(axis=0)


def filled_up(lines, devices):
    spare = -lines.shape[0] % devices
    if not spare:
        return lines
    return jnp.concatenate([lines, jnp.zeros((spare, *lines.shape[1:]), lines.dtype)])


def sent_to_all(array, axis):
    devices = lax.axis_size(axis)
    return lax.all_to_all(
        jnp.broadcast_to(array[None], (devices, *array.shape)), axis, 0, 0, tiled=True
    )


def in_order(parts, dim):
    dims = list(parts.shape[1:])
    dims[dim] *= parts.shape[0]
    return jnp.moveaxis(parts, 0, dim).reshape(dims)


def gathered_by_axis(array, axes, dim):
    far, near = axes
    initial = sent_to_all(array, far)
    parts = jnp.swapaxes(sent_to_all(initial, near), 0, 1)
    return in_order(parts.reshape(-1, *array.shape), dim)


def sum_by_parts(array, axes):
    lines = array.reshape(-1, array.shape[-1])
    own = sum_in_two_steps(
        filled_up(lines, lax.axis_size(axes[0]) * lax.axis_size(axes[1])), axes, 0
    )
    whole = gathered_by_axis(own, axes, 0)
    return whole[: len(lines)].reshape(array.shape)


def gather_axes(array, axes, dim):
    if not axes:
        return array
    nearer = lax.all_gather(array, axes[-1], axis=dim, tiled=True)
    return gather_axes(nearer, axes[:-1], dim)


def collect(array, axis, dim):
    parts = sent_to_all(array, axis)
    return in_order(parts, dim)


def over_copies(array, axis):
    everything = sent_to_all(array, axis)
    return jnp.sum(everything, axis=0)


def by_axis(array, axes):
    far, near = axes
    nearer = over_copies(array, near)
    return over_copies(nearer, far)


def adam_direction(moment_one, moment_two, gradient):
    mean_new = BETA_ONE * moment_one + (1.0 - BETA_ONE) * gradient
    second_new = BETA_TWO * moment_two + (1.0 - BETA_TWO) * gradient * gradient
    return (mean_new, second_new, mean_new / (jnp.sqrt(second_new) + ADAM_EPS))


def block_sum(left_parts, right_side):
    tp_count = lax.axis_size(TP)
    result = jnp.zeros(
        (right_side.shape[1] // tp_count * lax.axis_size(TP), left_parts[0].shape[1]), jnp.float32
    )
    for left_side in left_parts:
        result = result + lax.dot_general(
            right_side, left_side, TOKEN_DIMS, preferred_element_type=jnp.float32
        )
    column_block = sum_in_two_steps(result, ("tp_0", "tp_1"), 0)
    return sent_and_summed(column_block, FS, 1).T


def local(
    saved_input,
    value_cotangent,
    decay_cotangent,
    value_master,
    value_factor,
    value_mean,
    value_second,
    decay_master,
    decay_mean,
    decay_second,
):
    decay_local = lax.dot_general(
        saved_input, decay_cotangent, TOKEN_DIMS, preferred_element_type=jnp.float32
    )
    decay_grad = sum_by_parts(decay_local, (("fs_0", "fs_1"), ("tp_0", "tp_1")))
    unused_mean, unused_second, decay_step = adam_direction(decay_mean, decay_second, decay_grad)
    decay_copy = (decay_master - LEARN_RATE * decay_step).astype(jnp.bfloat16)
    factor_wide = value_factor.astype(jnp.float32)
    mapped = jnp.dot(
        saved_input, gather_axes(value_factor, FS, 0), preferred_element_type=jnp.float32
    )
    high_part = lax.optimization_barrier(mapped.astype(jnp.bfloat16))
    low_part = (mapped - high_part.astype(jnp.float32)).astype(jnp.bfloat16)
    projected = block_sum((high_part, low_part), value_cotangent)
    mean_new, second_new, direction = adam_direction(value_mean, value_second, projected)
    raw_update = jnp.dot(
        factor_wide,
        collect(direction, FS, 0),
        precision=lax.Precision.HIGHEST,
        preferred_element_type=jnp.float32,
    )
    squares = by_axis(jnp.sum(raw_update * raw_update), (("fs_0", "fs_1"), ("tp_0", "tp_1")))
    value_step = raw_update * lax.rsqrt(squares / (D * GW) + RMS_EPS)
    value_new = value_master - LEARN_RATE * value_step
    value_copy = collect(value_new.astype(jnp.bfloat16), FS, 0)
    return (value_step, value_new, value_copy, mean_new, second_new, decay_step, decay_copy)


def solution(mesh):
    split = Mesh(mesh.devices.reshape(8, 4, 4, 2), ("fs_0", "fs_1", "tp_0", "tp_1"))
    return jax.shard_map(
        local,
        mesh=split,
        in_specs=(
            P(FS_TP, None),
            P(FS_TP, None),
            P(FS_TP, None),
            P(FS, TP),
            P(FS, None),
            P(FS, TP),
            P(FS, TP),
            P(),
            P(),
            P(),
        ),
        out_specs=(P(FS, TP), P(FS, TP), P(None, TP), P(FS, TP), P(FS, TP), P(), P()),
        check_vma=False,
    )
```

profile of v0, /device:TPU:1, one launch (start us, length us, event | category | flops | bytes accessed | tf_op | source)
XLA Modules:
  0.0 228.8 jit_solution(8956926485409966899)
XLA Ops:
  7.2 12.3 %all_gather.6 = bf16[256,256]{1,0:T(8,128)(2,1)} all-gather(bf16[64,256]{1,0:T(8,128)(2,1)} %param.14), channel_id=1, replica_groups=mesh['fs_0'=8,'fs_1'=4,'tp_0'=4,'tp_1'=2] {'fs_1'}, dimensions={0}, use_global_device_ids=true | all-gather | bytes 163840 | tf_op jit(solution)/shard_map/all_gather | solution.py:81
  19.5 5.7 %fusion.15 = f32[2048,16]{1,0:T(8,128)} fusion(bf16[1536,2048]{1,0:T(8,128)(2,1)} %param.10, bf16[1536,16]{0,1:T(8,128)(2,1)} %param.12), kind=kOutput, calls=%fused_computation.26 | convolution fusion | flops 100663296 | bytes 6471680 | tf_op jit(solution)/shard_map/dot_general | solution.py:132
  29.7 27.7 %all-gather.2.cloned.1.call-done = bf16[2048,256]{1,0:T(8,128)(2,1)} async-done(((bf16[256,256]{1,0:T(8,128)(2,1)}), bf16[2048,256]{1,0:T(8,128)(2,1)}) %all-gather.2.cloned.1.call-update) | async-done | bytes 1048592 | tf_op jit(solution)/shard_map/all_gather | solution.py:81
  57.4 5.0 %fusion.13 = (bf16[1536,256]{1,0:T(8,128)(2,1)S(1)}, f32[1536,256]{1,0:T(8,128)S(1)}) fusion(bf16[1536,2048]{1,0:T(8,128)(2,1)} %param.10, bf16[2048,256]{1,0:T(8,128)(2,1)} %all-gather.2.cloned.1.call-done), kind=kOutput, calls=%fused_computation.21 | convolution fusion | flops 1611005952 | bytes 9699328 | tf_op jit(solution)/shard_map/dot_general | solution.py:139
  65.4 3.1 %reshape_reshape.9 = f32[4,2,128,256]{2,1,0,3:T(2,128)} reshape(f32[1024,256]{0,1:T(8,128)} %fusion) | data formatting | bytes 2097152 | tf_op jit(solution)/shard_map/reshape;reshape | solution.py:24
  70.1 10.7 %all_to_all.57 = f32[2,4,128,256]{2,1,3,0:T(4,128)} all-to-all(f32[2,4,128,256]{2,1,3,0:T(4,128)S(1)} %bitcast.49), channel_id=1, replica_groups=mesh['fs_0'=8,'fs_1'=4,'tp_0'=4,'tp_1'=2] {'tp_1'}, dimensions={0} | all-to-all | bytes 2097152 | tf_op jit(solution)/shard_map/all_to_all | solution.py:30
  80.8 4.7 %all-to-all-start.7 = ((f32[8,1,4096]{2,1,0:T(1,128)}), f32[8,1,4096]{2,1,0:T(1,128)S(1)}, u32[]{:S(2)}, u32[]{:S(2)}) async-start(f32[8,1,4096]{2,1,0:T(1,128)} %reshape.36), calls=%async_computation.7 | async-start | bytes 262144 | tf_op jit(solution)/shard_map/all_to_all | solution.py:30
  90.7 4.1 %all-to-all-start.1 = ((f32[4,128,256]{1,2,0:T(8,128)}), f32[4,128,256]{1,2,0:T(8,128)}, u32[]{:S(2)}, u32[]{:S(2)}) async-start(f32[4,128,256]{1,2,0:T(8,128)} %copy.100), calls=%async_computation.1 | async-start | bytes 1048576 | tf_op jit(solution)/shard_map/all_to_all | solution.py:38
  99.2 4.4 %all-to-all-done.1 = f32[4,128,256]{1,2,0:T(8,128)} async-done(((f32[4,128,256]{1,2,0:T(8,128)}), f32[4,128,256]{1,2,0:T(8,128)}, u32[]{:S(2)}, u32[]{:S(2)}) %all-to-all-start.1) | async-done | bytes 524320 | tf_op jit(solution)/shard_map/all_to_all | solution.py:38
  103.6 6.6 %all-to-all-start.8 = ((f32[32,1,128]{2,1,0:T(1,128)}), f32[32,1,128]{2,1,0:T(1,128)S(1)}, u32[]{:S(2)}, u32[]{:S(2)}) async-start(f32[32,1,128]{2,1,0:T(1,128)} %reshape.38), calls=%async_computation.8 | async-start | bytes 32768 | tf_op jit(solution)/shard_map/all_to_all | solution.py:38
  112.0 6.8 %all-to-all-done.8 = f32[32,1,128]{2,1,0:T(1,128)S(1)} async-done(((f32[32,1,128]{2,1,0:T(1,128)}), f32[32,1,128]{2,1,0:T(1,128)S(1)}, u32[]{:S(2)}, u32[]{:S(2)}) %all-to-all-start.8) | async-done | bytes 16416 | tf_op jit(solution)/shard_map/all_to_all | solution.py:38
  118.8 3.9 %all-to-all-start.2 = ((f32[32,128,8]{1,2,0:T(8,128)}), f32[32,128,8]{1,2,0:T(8,128)S(1)}, u32[]{:S(2)}, u32[]{:S(2)}) async-start(f32[32,128,8]{1,2,0:T(8,128)} %bitcast.3), calls=%async_computation.2 | async-start | bytes 262144 | tf_op jit(solution)/shard_map/all_to_all | solution.py:30
  124.2 7.9 %all-to-all-done.2 = f32[32,128,8]{1,2,0:T(8,128)S(1)} async-done(((f32[32,128,8]{1,2,0:T(8,128)}), f32[32,128,8]{1,2,0:T(8,128)S(1)}, u32[]{:S(2)}, u32[]{:S(2)}) %all-to-all-start.2) | async-done | bytes 131104 | tf_op jit(solution)/shard_map/all_to_all | solution.py:30
  132.1 3.8 %all-to-all-start.9 = ((f32[32,1,128]{2,1,0:T(1,128)}), f32[32,1,128]{2,1,0:T(1,128)S(1)}, u32[]{:S(2)}, u32[]{:S(2)}) async-start(f32[32,1,128]{2,1,0:T(1,128)} %reshape.40), calls=%async_computation.9 | async-start | bytes 32768 | tf_op jit(solution)/shard_map/all_to_all | solution.py:51
  136.6 7.9 %all-to-all-done.9 = f32[32,1,128]{2,1,0:T(1,128)S(1)} async-done(((f32[32,1,128]{2,1,0:T(1,128)}), f32[32,1,128]{2,1,0:T(1,128)S(1)}, u32[]{:S(2)}, u32[]{:S(2)}) %all-to-all-start.9) | async-done | bytes 16416 | tf_op jit(solution)/shard_map/all_to_all | solution.py:51
  145.1 3.9 %all-to-all-start.3 = ((f32[32,8,128]{2,1,0:T(8,128)}), f32[32,8,128]{2,1,0:T(8,128)S(1)}, u32[]{:S(2)}, u32[]{:S(2)}) async-start(f32[32,8,128]{2,1,0:T(8,128)} %broadcast_in_dim.12), calls=%async_computation.3 | async-start | bytes 262144 | tf_op jit(solution)/shard_map/all_to_all | solution.py:51
  149.9 8.5 %all-to-all-done.3 = f32[32,8,128]{2,1,0:T(8,128)S(1)} async-done(((f32[32,8,128]{2,1,0:T(8,128)}), f32[32,8,128]{2,1,0:T(8,128)S(1)}, u32[]{:S(2)}, u32[]{:S(2)}) %all-to-all-start.3) | async-done | bytes 131104 | tf_op jit(solution)/shard_map/all_to_all | solution.py:51
  159.8 13.6 %all_to_all.58 = f32[8,1,1]{2,1,0:T(1,128)S(1)} all-to-all(f32[8,1,1]{2,1,0:T(1,128)S(1)} %broadcast_in_dim.13), channel_id=1, replica_groups=mesh['fs_0'=8,'fs_1'=4,'tp_0'=4,'tp_1'=2] {'tp_0','tp_1'}, dimensions={0} | all-to-all | bytes 64 | tf_op jit(solution)/shard_map/all_to_all | solution.py:51
  175.3 4.0 %all-to-all-start.5 = ((f32[32,1,1]{2,1,0:T(1,128)}), f32[32,1,1]{2,1,0:T(1,128)S(1)}, u32[]{:S(2)}, u32[]{:S(2)}) async-start(f32[32,1,1]{2,1,0:T(1,128)} %broadcast_in_dim.14), calls=%async_computation.5 | async-start | bytes 32768 | tf_op jit(solution)/shard_map/all_to_all | solution.py:51
  182.1 5.8 %all-to-all-done.5 = f32[32,1,1]{2,1,0:T(1,128)S(1)} async-done(((f32[32,1,1]{2,1,0:T(1,128)}), f32[32,1,1]{2,1,0:T(1,128)S(1)}, u32[]{:S(2)}, u32[]{:S(2)}) %all-to-all-start.5) | async-done | bytes 160 | tf_op jit(solution)/shard_map/all_to_all | solution.py:51
  187.9 5.1 %all-to-all-start.10 = ((f32[8,1,4096]{2,1,0:T(1,128)}), f32[8,1,4096]{2,1,0:T(1,128)S(1)}, u32[]{:S(2)}, u32[]{:S(2)}) async-start(f32[8,1,4096]{2,1,0:T(1,128)} %reshape.42), calls=%async_computation.10 | async-start | bytes 262144 | tf_op jit(solution)/shard_map/all_to_all | solution.py:51
  194.9 3.3 %all-to-all-done.10 = f32[8,1,4096]{2,1,0:T(1,128)S(1)} async-done(((f32[8,1,4096]{2,1,0:T(1,128)}), f32[8,1,4096]{2,1,0:T(1,128)S(1)}, u32[]{:S(2)}, u32[]{:S(2)}) %all-to-all-start.10) | async-done | bytes 131104 | tf_op jit(solution)/shard_map/all_to_all | solution.py:51
  199.1 4.6 %all-to-all-start.6 = ((bf16[32,64,128]{2,1,0:T(8,128)(2,1)}), bf16[32,64,128]{2,1,0:T(8,128)(2,1)}, u32[]{:S(2)}, u32[]{:S(2)}) async-start(bf16[32,64,128]{2,1,0:T(8,128)(2,1)} %broadcast_in_dim.15), calls=%async_computation.6 | async-start | bytes 1048576 | tf_op jit(solution)/shard_map/all_to_all | solution.py:51
  213.6 6.4 %all-to-all-done.6 = bf16[32,64,128]{2,1,0:T(8,128)(2,1)} async-done(((bf16[32,64,128]{2,1,0:T(8,128)(2,1)}), bf16[32,64,128]{2,1,0:T(8,128)(2,1)}, u32[]{:S(2)}, u32[]{:S(2)}) %all-to-all-start.6) | async-done | bytes 524320 | tf_op jit(solution)/shard_map/all_to_all | solution.py:51
  (58 shorter events, 44.1 us)
Async XLA Ops:
  7.2 55.2 %copy-start = (bf16[1536,1024]{1,0:T(8,128)(2,1)S(1)}, bf16[1536,1024]{1,0:T(8,128)(2,1)}, u32[]{:S(2)}) copy-start(bf16[1536,1024]{1,0:T(8,128)(2,1)} %param.11) | copy-start | bytes 9437188
  7.2 50.2 %all-gather.2.cloned.1.call-start = ((), (), s32[]{:S(2)}) async-start(), calls=%async_computation.11 | async-start | bytes 1179648 | tf_op jit(solution)/shard_map/all_gather | solution.py:81
  80.8 9.9 %all-to-all-start.7 = ((f32[8,1,4096]{2,1,0:T(1,128)}), f32[8,1,4096]{2,1,0:T(1,128)S(1)}, u32[]{:S(2)}, u32[]{:S(2)}) async-start(f32[8,1,4096]{2,1,0:T(1,128)} %reshape.36), calls=%async_computation.7 | async-start | bytes 262144 | tf_op jit(solution)/shard_map/all_to_all | solution.py:30
  87.8 48.1 %copy-start.5 = (f32[8,128]{1,0:T(8,128)S(1)}, f32[8,128]{1,0:T(8,128)}, u32[]{:S(2)}) copy-start(f32[8,128]{1,0:T(8,128)} %param.16) | copy-start | bytes 12292
  87.8 48.1 %copy-start.6 = (f32[8,128]{1,0:T(8,128)S(1)}, f32[8,128]{1,0:T(8,128)}, u32[]{:S(2)}) copy-start(f32[8,128]{1,0:T(8,128)} %param.15) | copy-start | bytes 12292
  87.9 70.5 %copy-start.1 = (bf16[64,256]{1,0:T(8,128)(2,1)S(1)}, bf16[64,256]{1,0:T(8,128)(2,1)}, u32[]{:S(2)}) copy-start(bf16[64,256]{1,0:T(8,128)(2,1)} %param.14) | copy-start | bytes 98308
  90.7 12.9 %all-to-all-start.1 = ((f32[4,128,256]{1,2,0:T(8,128)}), f32[4,128,256]{1,2,0:T(8,128)}, u32[]{:S(2)}, u32[]{:S(2)}) async-start(f32[4,128,256]{1,2,0:T(8,128)} %copy.100), calls=%async_computation.1 | async-start | bytes 1048576 | tf_op jit(solution)/shard_map/all_to_all | solution.py:38
  94.8 99.5 %copy-start.4 = (f32[64,128]{1,0:T(8,128)S(1)}, f32[64,128]{1,0:T(8,128)}, u32[]{:S(2)}) copy-start(f32[64,128]{1,0:T(8,128)} %param.13) | copy-start | bytes 98308
  103.6 15.2 %all-to-all-start.8 = ((f32[32,1,128]{2,1,0:T(1,128)}), f32[32,1,128]{2,1,0:T(1,128)S(1)}, u32[]{:S(2)}, u32[]{:S(2)}) async-start(f32[32,1,128]{2,1,0:T(1,128)} %reshape.38), calls=%async_computation.8 | async-start | bytes 32768 | tf_op jit(solution)/shard_map/all_to_all | solution.py:38
  118.8 13.3 %all-to-all-start.2 = ((f32[32,128,8]{1,2,0:T(8,128)}), f32[32,128,8]{1,2,0:T(8,128)S(1)}, u32[]{:S(2)}, u32[]{:S(2)}) async-start(f32[32,128,8]{1,2,0:T(8,128)} %bitcast.3), calls=%async_computation.2 | async-start | bytes 262144 | tf_op jit(solution)/shard_map/all_to_all | solution.py:30
  132.1 12.4 %all-to-all-start.9 = ((f32[32,1,128]{2,1,0:T(1,128)}), f32[32,1,128]{2,1,0:T(1,128)S(1)}, u32[]{:S(2)}, u32[]{:S(2)}) async-start(f32[32,1,128]{2,1,0:T(1,128)} %reshape.40), calls=%async_computation.9 | async-start | bytes 32768 | tf_op jit(solution)/shard_map/all_to_all | solution.py:51
  145.1 13.3 %all-to-all-start.3 = ((f32[32,8,128]{2,1,0:T(8,128)}), f32[32,8,128]{2,1,0:T(8,128)S(1)}, u32[]{:S(2)}, u32[]{:S(2)}) async-start(f32[32,8,128]{2,1,0:T(8,128)} %broadcast_in_dim.12), calls=%async_computation.3 | async-start | bytes 262144 | tf_op jit(solution)/shard_map/all_to_all | solution.py:51
  175.3 12.6 %all-to-all-start.5 = ((f32[32,1,1]{2,1,0:T(1,128)}), f32[32,1,1]{2,1,0:T(1,128)S(1)}, u32[]{:S(2)}, u32[]{:S(2)}) async-start(f32[32,1,1]{2,1,0:T(1,128)} %broadcast_in_dim.14), calls=%async_computation.5 | async-start | bytes 32768 | tf_op jit(solution)/shard_map/all_to_all | solution.py:51
  187.9 10.4 %all-to-all-start.10 = ((f32[8,1,4096]{2,1,0:T(1,128)}), f32[8,1,4096]{2,1,0:T(1,128)S(1)}, u32[]{:S(2)}, u32[]{:S(2)}) async-start(f32[8,1,4096]{2,1,0:T(1,128)} %reshape.42), calls=%async_computation.10 | async-start | bytes 262144 | tf_op jit(solution)/shard_map/all_to_all | solution.py:51
  198.2 13.7 %copy-start.2 = (f32[2048,16]{0,1:T(8,128)S(1)}, f32[2048,16]{0,1:T(8,128)}, u32[]{:S(2)}) copy-start(f32[2048,16]{0,1:T(8,128)} %param.17) | copy-start | bytes 393220
  199.1 20.9 %all-to-all-start.6 = ((bf16[32,64,128]{2,1,0:T(8,128)(2,1)}), bf16[32,64,128]{2,1,0:T(8,128)(2,1)}, u32[]{:S(2)}, u32[]{:S(2)}) async-start(bf16[32,64,128]{2,1,0:T(8,128)(2,1)} %broadcast_in_dim.15), calls=%async_computation.6 | async-start | bytes 1048576 | tf_op jit(solution)/shard_map/all_to_all | solution.py:51
  204.7 7.2 %copy-start.3 = (f32[2048,16]{0,1:T(8,128)S(1)}, f32[2048,16]{0,1:T(8,128)}, u32[]{:S(2)}) copy-start(f32[2048,16]{0,1:T(8,128)} %param.19) | copy-start | bytes 393220
Sparse Core Ops, SparseCore 0:
  19.7 37.6 all-gather.1
where the time goes:
time: 230 us; the launch traced here: 229 us
  waiting for transfers between devices  79.6 us (35%)
  starting transfers between devices  40.8 us (18%)
  blocking collectives  36.6 us (16%)
  local copies, waits for them, and re-layouts  29.7 us (13%)
  between operations  14.9 us (6%)
  matrix products  14.5 us (6%)
  other arithmetic  12.7 us (6%)
    all_to_all x5, waiting for transfers between devices, sent_to_all(): lax.all_to_all(jnp.broadcast_to(array[None], (devices, *array.shape)), ax...  31.9 us
    all_gather x1, waiting for transfers between devices, gather_axes(): nearer = lax.all_gather(array, axes[-1], axis=dim, tiled=True)  27.7 us
    all_to_all x5, starting transfers between devices, sent_to_all(): lax.all_to_all(jnp.broadcast_to(array[None], (devices, *array.shape)), ax...  21.4 us
    all_to_all x1, blocking collectives, sent_to_all(): lax.all_to_all(jnp.broadcast_to(array[None], (devices, *array.shape)), ax...  13.6 us
    all_gather x1, blocking collectives, gather_axes(): nearer = lax.all_gather(array, axes[-1], axis=dim, tiled=True)  12.3 us
    all_to_all x2, waiting for transfers between devices, sum_in_two_steps(): lax.all_to_all(nearer, far, split_axis=0, concat_axis=0, tiled=True)  11.2 us
    all_to_all x2, starting transfers between devices, sum_in_two_steps(): lax.all_to_all(nearer, far, split_axis=0, concat_axis=0, tiled=True)  10.8 us
    all_to_all x1, blocking collectives, sent_and_summed(): lax.all_to_all(parts, axis, split_axis=0, concat_axis=0, tiled=True)  10.7 us
  transfers between devices with their start and end apart: 10, of which 10 were waited for; matrix products, arithmetic and copies ran while one was open for 16% of the time, Pallas kernels for 0%

commit v1 on v0

v1 whole, which is shorter than its diff:
```python
import functools

import jax
import jax.numpy as jnp
from jax import lax
from jax.experimental import pallas as pl
from jax.experimental.pallas import tpu as pltpu
from jax.sharding import Mesh
from jax.sharding import PartitionSpec as P

MESH = pl.DeviceIdType.MESH
FS = ("fs_0", "fs_1")
TP = ("tp_0", "tp_1")
FS_TP = FS + TP
NZ, NX, NY, NC = 8, 4, 4, 2
D = 2048
GW = 1024
RANK = 256
HG = 16
TOK = 1536

BETA_ONE = 0.9
BETA_TWO = 0.99
ADAM_EPS = 1e-08
RMS_EPS = 1e-06
LEARN_RATE = 0.05

N_REMOTE = 7 + 6 + 8 + 7 + 3 + 24 + 4 + 3 + 3 + 7 + 7 + 3 + 7
F32 = jnp.float32
BF16 = jnp.bfloat16


def moments(mean, second, grad):
    mean_new = BETA_ONE * mean + (1.0 - BETA_ONE) * grad
    second_new = BETA_TWO * second + (1.0 - BETA_TWO) * grad * grad
    return mean_new, second_new, mean_new / (jnp.sqrt(second_new) + ADAM_EPS)


def split_two(value):
    high = value.astype(BF16)
    return high, (value - high.astype(F32)).astype(BF16)


def kernel(
    x_in, g_in, dct_in, master_in, f_in, mean_in, second_in, dmaster_in, dmean_in, dsecond_in,
    step_out, new_out, copy_out, mean_out, second_out, dstep_out, dcopy_out,
    xv, gv, dctv, fv, mv, meanv, secondv, dmasterv, dmeanv, dsecondv,
    mapped, split_t, pbuf, crecv, yrecv, sbuf, xrecv, tbuf, zrecv, dirb, ubuf, sqb,
    dacc, dbuf, dcrecv, dyrecv, dsend, dxrecv, dzall, dgrad,
    stepv, newv, copyv, dstepv, dcopyv,
    local_sem, send_sem, recv_sem,
):
    z = lax.axis_index("fs_0")
    x = lax.axis_index("fs_1")
    y = lax.axis_index("tp_0")
    c = lax.axis_index("tp_1")
    tp = y * NC + c
    mate = 1 - c
    half = pl.ds(pl.multiple_of(c * 32, 32), 32)

    def z_at(k):
        return {"fs_0": lax.rem(z + k, NZ)}

    def x_at(k):
        return {"fs_1": lax.rem(x + k, NX)}

    def y_at(k):
        return {"tp_0": lax.rem(y + k, NY)}

    def tp_at(k):
        other = lax.rem(tp + k, NY * NC)
        return {"tp_0": other // NC, "tp_1": lax.rem(other, NC)}

    core = {"tp_1": mate}
    z_far = (4, 3, 5, 2, 6, 1, 7)
    x_far = (2, 1, 3)

    locals_started = []
    sends = []

    def fetch(src, dst):
        copy = pltpu.make_async_copy(src, dst, local_sem.at[len(locals_started)])
        copy.start()
        locals_started.append(copy)
        return copy

    def send(src, dst, where):
        n = len(sends)
        copy = pltpu.make_async_remote_copy(
            src_ref=src, dst_ref=dst, send_sem=send_sem.at[n], recv_sem=recv_sem.at[n],
            device_id=where, device_id_type=MESH,
        )
        copy.start()
        sends.append(copy)
        return copy

    own_f = fetch(f_in.at[half], fv.at[z, x, half])
    dct_load = fetch(dct_in, dctv)
    x_loads = [
        fetch(x_in.at[pl.ds(512 * i, 512)], xv.at[pl.ds(512 * i, 512)]) for i in range(3)
    ]
    own_m = fetch(master_in, mv.at[z, x])
    g_load = fetch(g_in, gv)
    small_loads = [
        fetch(mean_in, meanv), fetch(second_in, secondv), fetch(dmaster_in, dmasterv),
        fetch(dmean_in, dmeanv), fetch(dsecond_in, dsecondv),
    ]

    barrier = pltpu.get_barrier_semaphore()
    peers = [z_at(k) for k in z_far] + [x_at(k) for k in x_far]
    peers += [tp_at(k) for k in range(1, 8)]
    for peer in peers:
        pl.semaphore_signal(barrier, inc=1, device_id=peer, device_id_type=MESH)
    pl.semaphore_wait(barrier, len(peers))

    own_f.wait()
    f_z = [send(fv.at[z, x, half], fv.at[z, x, half], z_at(k)) for k in z_far]

    dct_load.wait()
    for i in range(3):
        x_loads[i].wait()
        part = jnp.dot(
            dctv[:, 512 * i : 512 * (i + 1)], xv[512 * i : 512 * (i + 1), :],
            preferred_element_type=F32,
        )
        if i < 2:
            dacc[...] = part if i == 0 else dacc[...] + part
        else:
            part = dacc[...] + part
            for t in range(NY * NC):
                for q in range(NX):
                    row, col = 8 * (q // 2), 256 * t + 128 * (q % 2)
                    dbuf[t // NC, t % NC, q] = part[row : row + 8, col : col + 128]
    d_core = send(dbuf.at[:, mate], dcrecv, core)

    for copy in f_z:
        copy.wait_recv()
    zs = [pl.ds(4 * h, 4) for h in range(2)]
    f_x = [
        [send(fv.at[zs[h], x, half], fv.at[zs[h], x, half], x_at(k)) for k in x_far]
        for h in range(2)
    ]
    f_c = [[send(fv.at[zs[h], x, half], fv.at[zs[h], x, half], core)] for h in range(2)]

    d_core.wait_recv()
    for t in range(NY):
        dbuf[t, c] = dbuf[t, c] + dcrecv[t]
    d_y = [
        send(dbuf.at[lax.rem(y + k, NY), c], dyrecv.at[k - 1], y_at(k)) for k in (2, 1, 3)
    ]
    own_m.wait()
    m_z = [send(mv.at[z, x], mv.at[z, x], z_at(k)) for k in z_far]

    for copy in d_y:
        copy.wait_recv()
    dsend[...] = dbuf[y, c] + dyrecv[0] + dyrecv[1] + dyrecv[2]
    d_x = [send(dsend.at[lax.rem(x + k, NX)], dxrecv.at[k - 1], x_at(k)) for k in x_far]

    for h in range(2):
        for k in range(3):
            f_x[h][k].wait_recv()
            source = lax.rem(x + NX - x_far[k], NX)
            piece = fv.at[zs[h], source, half]
            f_c[h].append(send(piece, piece, core))
        if h == 0:
            for copy in d_x:
                copy.wait_recv()
            dzall[z] = dsend[x] + dxrecv[0] + dxrecv[1] + dxrecv[2]
            d_z = [send(dzall.at[z], dzall.at[z], z_at(k)) for k in z_far]
        for copy in f_c[h]:
            copy.wait_recv()

        def tile(i, carry):
            rows = pl.ds(pl.multiple_of(i * 256, 256), 256)
            factor = fv[4 * h : 4 * h + 4].reshape(1024, RANK)
            part = jnp.dot(
                xv[rows, 1024 * h : 1024 * (h + 1)], factor, preferred_element_type=F32
            )
            if h == 0:
                mapped[rows, :] = part
            else:
                high, low = split_two((mapped[rows, :] + part).T)
                split_t[0:256, rows] = high
                split_t[256:512, rows] = low
            return carry

        lax.fori_loop(0, TOK // 256, tile, 0)

    for copy in m_z:
        copy.wait_recv()
    m_x = [send(mv.at[:, x], mv.at[:, x], x_at(k)) for k in x_far]

    g_load.wait()
    order = (2, 1, 3, 0)
    p_c = []
    p_y = []

    def pass_on(n):
        k = order[n]
        target = lax.rem(y + k, NY)
        p_c[n].wait_recv()
        pbuf[target, c] = pbuf[target, c] + crecv[n]
        if k:
            p_y.append(send(pbuf.at[target, c], yrecv.at[k - 1], y_at(k)))

    for n in range(NY):
        target = lax.rem(y + order[n], NY)
        both = jnp.dot(
            split_t[...], gv[:, pl.ds(pl.multiple_of(target * 256, 256), 256)],
            preferred_element_type=F32,
        )
        part = both[:RANK] + both[RANK:]
        pbuf[target, 0] = part[:, :128]
        pbuf[target, 1] = part[:, 128:]
        p_c.append(send(pbuf.at[target, mate], crecv.at[n], core))
        if n >= 2:
            pass_on(n - 2)
    pass_on(2)
    pass_on(3)

    for copy in d_z:
        copy.wait_recv()
    total = dzall[0]
    for k in range(1, NZ):
        total = total + dzall[k]
    dgrad[tp, x] = total
    d_ax = [send(dgrad.at[tp, x], dgrad.at[tp, x], x_at(k)) for k in x_far]

    for copy in p_y:
        copy.wait_recv()
    total = pbuf[y, c] + yrecv[0] + yrecv[1] + yrecv[2]
    sbuf[...] = total.reshape(NZ, NX, 8, 128)
    p_x = [send(sbuf.at[:, lax.rem(x + k, NX)], xrecv.at[k - 1], x_at(k)) for k in x_far]

    for copy in d_ax:
        copy.wait_recv()
    d_at = [send(dgrad.at[tp], dgrad.at[tp], tp_at(k)) for k in range(1, 8)]

    for copy in p_x:
        copy.wait_recv()
    tbuf[...] = sbuf[:, x] + xrecv[0] + xrecv[1] + xrecv[2]
    p_z = [send(tbuf.at[lax.rem(z + k, NZ)], zrecv.at[k - 1], z_at(k)) for k in z_far]
    for copy in small_loads:
        copy.wait()
    for copy in p_z:
        copy.wait_recv()
    projected = tbuf[z]
    for k in range(NZ - 1):
        projected = projected + zrecv[k]
    mean_new, second_new, direction = moments(meanv[...], secondv[...], projected)
    dirb[z, x] = direction
    a_z = [send(dirb.at[z, x], dirb.at[z, x], z_at(k)) for k in z_far]
    meanv[...] = mean_new
    secondv[...] = second_new
    outs = [fetch(meanv, mean_out), fetch(secondv, second_out)]

    for copy in d_at:
        copy.wait_recv()
    for t in range(NY * NC):
        for q in range(2):
            cols = slice(256 * t + 128 * q, 256 * t + 128 * (q + 1))
            grad = jnp.concatenate([dgrad[t, q], dgrad[t, 2 + q]], axis=0)
            _, _, step = moments(dmeanv[:, cols], dsecondv[:, cols], grad)
            dstepv[:, cols] = step
            dcopyv[:, cols] = (dmasterv[:, cols] - LEARN_RATE * step).astype(BF16)
    outs += [fetch(dstepv, dstep_out), fetch(dcopyv, dcopy_out)]

    for copy in a_z:
        copy.wait_recv()
    a_x = [send(dirb.at[:, x], dirb.at[:, x], x_at(k)) for k in x_far]
    for copy in m_x:
        copy.wait_recv()
    for copy in a_x:
        copy.wait_recv()

    high, low = split_two(dirb[...].reshape(RANK, 128))
    rhs = jnp.concatenate([high, low], axis=1)
    squares = jnp.zeros((8, 128), F32)
    for i in range(NZ):
        both = jnp.dot(fv[i].reshape(256, RANK), rhs, preferred_element_type=F32)
        part = both[:, :128] + both[:, 128:]
        ubuf[256 * i : 256 * (i + 1), :] = part
        squares = squares + jnp.sum((part * part).reshape(32, 8, 128), axis=0)
    sqb[tp] = squares
    s_t = [send(sqb.at[tp], sqb.at[tp], tp_at(k)) for k in range(1, 8)]
    for copy in s_t:
        copy.wait_recv()
    whole = sqb[0]
    for k in range(1, NY * NC):
        whole = whole + sqb[k]
    mean_square = jnp.sum(whole, axis=(0, 1), keepdims=True) / (D * GW)
    scale = lax.rsqrt(mean_square + RMS_EPS)
    fs = z * NX + x
    step = ubuf[pl.ds(pl.multiple_of(fs * 64, 64), 64), :] * scale
    stepv[...] = step
    newv[...] = mv[z, x] - LEARN_RATE * step
    outs += [fetch(stepv, step_out), fetch(newv, new_out)]
    for i in range(NZ):
        rows = slice(256 * i, 256 * (i + 1))
        step = ubuf[rows, :] * scale
        copyv[rows, :] = (mv[i].reshape(256, 128) - LEARN_RATE * step).astype(BF16)
    outs += [fetch(copyv, copy_out)]
    for copy in sends:
        copy.wait_send()
    for copy in outs:
        copy.wait()


def local(
    saved_input, value_cotangent, decay_cotangent, value_master, value_factor, value_mean,
    value_second, decay_master, decay_mean, decay_second,
):
    shape = jax.ShapeDtypeStruct
    any_spec = pl.BlockSpec(memory_space=pl.ANY)
    scratch = [
        ((TOK, D), BF16), ((TOK, GW), BF16), ((HG, TOK), BF16), ((NZ, NX, 64, RANK), BF16),
        ((NZ, NX, 64, 128), F32), ((8, 128), F32), ((8, 128), F32),
        ((HG, D), F32), ((HG, D), F32), ((HG, D), F32),
        ((TOK, RANK), F32), ((2 * RANK, TOK), BF16), ((NY, NC, RANK, 128), F32),
        ((NY, RANK, 128), F32), ((NY - 1, RANK, 128), F32), ((NZ, NX, 8, 128), F32),
        ((NX - 1, NZ, 8, 128), F32), ((NZ, 8, 128), F32), ((NZ - 1, 8, 128), F32),
        ((NZ, NX, 8, 128), F32), ((D, 128), F32), ((NY * NC, 8, 128), F32),
        ((HG, D), F32), ((NY, NC, NX, 8, 128), F32), ((NY, NX, 8, 128), F32),
        ((NY - 1, NX, 8, 128), F32), ((NX, 8, 128), F32), ((NX - 1, 8, 128), F32),
        ((NZ, 8, 128), F32), ((NY * NC, NX, 8, 128), F32),
        ((64, 128), F32), ((64, 128), F32), ((D, 128), BF16), ((HG, D), F32), ((HG, D), BF16),
    ]
    outs = pl.pallas_call(
        kernel,
        out_shape=(
            shape((64, 128), F32), shape((64, 128), F32), shape((D, 128), BF16),
            shape((8, 128), F32), shape((8, 128), F32), shape((HG, D), F32), shape((HG, D), BF16),
        ),
        in_specs=[any_spec] * 10,
        out_specs=(any_spec,) * 7,
        scratch_shapes=[pltpu.VMEM(*s) for s in scratch]
        + [
            pltpu.SemaphoreType.DMA((20,)),
            pltpu.SemaphoreType.DMA((N_REMOTE,)),
            pltpu.SemaphoreType.DMA((N_REMOTE,)),
        ],
        compiler_params=pltpu.CompilerParams(
            collective_id=0, has_side_effects=True, vmem_limit_bytes=56 * 1024 * 1024
        ),
    )(
        saved_input, value_cotangent, decay_cotangent.T, value_master, value_factor, value_mean,
        value_second, decay_master.T, decay_mean.T, decay_second.T,
    )
    return (*outs[:5], outs[5].T, outs[6].T)


def solution(mesh):
    split = Mesh(mesh.devices.reshape(NZ, NX, NY, NC), FS_TP)
    return jax.shard_map(
        local,
        mesh=split,
        in_specs=(
            P(FS_TP, None), P(FS_TP, None), P(FS_TP, None), P(FS, TP), P(FS, None), P(FS, TP),
            P(FS, TP), P(), P(), P(),
        ),
        out_specs=(P(FS, TP), P(FS, TP), P(None, TP), P(FS, TP), P(FS, TP), P(), P()),
        check_vma=False,
    )
```

time: 230 us -> 74.2 us (0.32)
  waiting for transfers between devices: 79.6 us -> 0 us
  Pallas kernels: 0 us -> 63 us
  starting transfers between devices: 40.8 us -> 0 us
  blocking collectives: 36.6 us -> 0 us
  local copies, waits for them, and re-layouts: 29.7 us -> 10.2 us
  matrix products: 14.5 us -> 0 us
  between operations: 14.9 us -> 0.65 us
  other arithmetic: 12.7 us -> 0 us
    pallas_call x0 -> x1, Pallas kernels: none -> 63 us  [local(): pl.pallas_call(kernel, out_shape=(shape((64, 128), F32), shape((64, 128),...]
    all_to_all x9 -> x0, waiting for transfers between devices: 51.9 us -> none  [the longest x5 31.9 us: sent_to_all(): lax.all_to_all(jnp.broadcast_to(array[None], (devices, *array.shape)), ax...]
    all_to_all x9 -> x0, starting transfers between devices: 40.7 us -> none  [the longest x5 21.4 us: sent_to_all(): lax.all_to_all(jnp.broadcast_to(array[None], (devices, *array.shape)), ax...]
    all_gather x1 -> x0, waiting for transfers between devices: 27.7 us -> none  [gather_axes(): nearer = lax.all_gather(array, axes[-1], axis=dim, tiled=True)]
    all_to_all x2 -> x0, blocking collectives: 24.3 us -> none  [the longest x1 13.6 us: sent_to_all(): lax.all_to_all(jnp.broadcast_to(array[None], (devices, *array.shape)), ax...]
    dot_general x5 -> x0, matrix products: 14.5 us -> none  [the longest x1 5.68 us: local(): lax.dot_general(saved_input, decay_cotangent, TOKEN_DIMS, preferred_eleme...]
    all_gather x1 -> x0, blocking collectives: 12.3 us -> none  [gather_axes(): nearer = lax.all_gather(array, axes[-1], axis=dim, tiled=True)]
    transpose x3 -> x0, local copies, waits for them, and re-layouts: 7.19 us -> none  [the longest x2 4.68 us: gathered_by_axis(): parts = jnp.swapaxes(sent_to_all(initial, near), 0, 1)]
  transfers between devices with their start and end apart: 10 -> 0, of which waited for: 10 -> 0; matrix products, arithmetic and copies ran while one was open for 16% -> 0% of each run, Pallas kernels for 0% -> 0%
where the time goes in v1:
time: 74.2 us; the launch traced here: 73.8 us
  Pallas kernels  63 us (85%)
  local copies, waits for them, and re-layouts  10.2 us (14%)
    pallas_call x1, Pallas kernels, local(): pl.pallas_call(kernel, out_shape=(shape((64, 128), F32), shape((64, 128),...  63 us
    unnamed x7, local copies, waits for them, and re-layouts  10.2 us

profile of v1, /device:TPU:1, one launch (start us, length us, event | category | flops | bytes accessed | tf_op | source)
XLA Modules:
  0.0 73.8 jit_solution(1352828673609943514)
XLA Ops:
  0.6 63.0 %shard_map.153 = (f32[64,128]{1,0:T(8,128)}, f32[64,128]{1,0:T(8,128)}, bf16[2048,128]{1,0:T(8,128)(2,1)}, f32[8,128]{1,0:T(8,128)}, f32[8,128]{1,0:T(8,128)}, /...) custom-call(bf16[1536,2048]{1,0:T(8,128)(2,1)} %x_in.1, bf16[1536,1024]{1,0:T(8,128)(2,1)} %g_in.1, ...), custom_call_target="tpu_custom_call" | custom-call | tf_op jit(solution)/shard_map/pallas_call | solution.py:328
  63.7 1.4 %copy.24 = f32[64,128]{1,0:T(8,128)} copy(f32[64,128]{1,0:T(8,128)} %get-tuple-element.28) | data formatting | bytes 65536
  65.0 1.4 %copy.25 = f32[64,128]{1,0:T(8,128)} copy(f32[64,128]{1,0:T(8,128)} %get-tuple-element.29) | data formatting | bytes 65536
  66.4 1.9 %copy.26 = bf16[2048,128]{1,0:T(8,128)(2,1)} copy(bf16[2048,128]{1,0:T(8,128)(2,1)} %get-tuple-element.30) | data formatting | bytes 1048576
  68.3 1.3 %copy.27 = f32[8,128]{1,0:T(8,128)} copy(f32[8,128]{1,0:T(8,128)} %get-tuple-element.31) | data formatting | bytes 8192
  69.5 1.3 %copy.28 = f32[8,128]{1,0:T(8,128)} copy(f32[8,128]{1,0:T(8,128)} %get-tuple-element.32) | data formatting | bytes 8192
  70.8 1.6 %copy.29 = f32[2048,16]{0,1:T(8,128)} copy(f32[2048,16]{0,1:T(8,128)} %bitcast.9) | data formatting | bytes 262144
  72.4 1.5 %copy.30 = bf16[2048,16]{0,1:T(8,128)(2,1)} copy(bf16[2048,16]{0,1:T(8,128)(2,1)} %bitcast.10) | data formatting | bytes 131072
